TPU v7x, 128 devices: a whole 4x4x4 slice. The times are simulated.
128 devices in a mesh: sp: 16 (over z, y), tp: 8 (over x, core).
Axes of the slice: x: 4, y: 4, z: 4, core: 2. Of those that a mesh axis runs over, the one named last changes fastest.
Arguments:
- tokens: bfloat16 [6144, 4096], P(('sp', 'tp')), may hold values from -6 to 6
- norm_gain: bfloat16 [4096], replicated, may hold values from 0.099609375 to 1.8984375
- w_pool_in: bfloat16 [4096, 4096], P('sp', 'tp'), may hold values from -0.09375 to 0.09375
- w_mem_in: bfloat16 [4096, 4096], P('sp', 'tp'), may hold values from -0.09375 to 0.09375
- w_input_gate: bfloat16 [4096, 16], replicated, may hold values from -104 to 104
- w_forget_gate: bfloat16 [4096, 16], replicated, may hold values from -0.09375 to 0.09375
- forget_bias: float32 [16], replicated, may hold values from 3 to 13
- forget_extra: float32 [6144, 16], P('sp', 'tp'), may hold values from 0 to 1.5
- conv_weight: bfloat16 [4, 4096], replicated, may hold values from -3 to 3
- query_map: bfloat16 [1024, 4, 4], replicated, may hold values from -3 to 3
- key_map: bfloat16 [1024, 4, 4], replicated, may hold values from -3 to 3
- pool_map: bfloat16 [16, 256, 256], P('tp'), may hold values from -0.375 to 0.375
- pool_gain: bfloat16 [4096], replicated, may hold values from 0.099609375 to 1.8984375
- mem_gain: bfloat16 [4096], replicated, may hold values from 0.099609375 to 1.8984375
- w_out_pool: bfloat16 [4096, 4096], P('tp', 'sp'), may hold values from -0.0625 to 0.0625
- w_out_mem: bfloat16 [4096, 4096], P('tp', 'sp'), may hold values from -0.0625 to 0.0625
Outputs:
- layer_out: bfloat16 [6144, 4096], P(('sp', 'tp'))
All inputs are finite; a program needn't handle non-finite values.
Results may differ from a plain program's by a relative error of at most 0.019.
The roundings to bfloat16 on the way count: a program that leaves them out, or rounds other values in their place, can miss the bound.
Values may be sent and summed in bfloat16 or wider, within the bound.
No kernel may reach another device: no remote copies, remote signals or barrier semaphores. Data moves between devices by JAX's collectives and lax.ppermute only.
A program may use at most 128 MiB of HBM per device.

v0:
```python
import jax
import jax.numpy as jnp
from jax import lax
from jax.sharding import Mesh
from jax.sharding import PartitionSpec as P

D = 4096
HEAD = 256
CONV = 4
BLOCK = 128
MEMORY_HEADS = 16
SP = ("sp_0", "sp_1")
SP_TP = ("sp_0", "sp_1", "tp")
epsilon = 1e-06
windows_all = (2, 4, 8, 16)
highest = lax.Precision.HIGHEST
lowest = -1e30


def rows_first(arrays, axis, dims):
    turned = [jnp.moveaxis(a, dim, 0) for a, dim in zip(arrays, dims)]
    both = jnp.concatenate([t.reshape(len(t), -1) for t in turned], axis=1)
    filled, at, gathered = (lax.all_gather(both, axis, axis=0, tiled=True), 0, [])
    for t, dim in zip(turned, dims):
        piece = filled[:, at : at + t[0].size].reshape(-1, *t.shape[1:])
        gathered.append(jnp.moveaxis(piece, 0, dim))
        at += t[0].size
    return tuple(gathered)


def in_one_piece(arrays, axis, dim, along):
    ends, at = ([], 0)
    for a in arrays[:-1]:
        at += a.shape[along]
        ends.append(at)
    both = jnp.concatenate(arrays, axis=along)
    return tuple(jnp.split(lax.all_gather(both, axis, axis=dim, tiled=True), ends, axis=along))


def passed_along(shard, axis, by):
    devices = lax.axis_size(axis)
    pairs = [(i, i + by) for i in range(devices) if 0 <= i + by < devices]
    return lax.ppermute(shard, axis, pairs)


def neutral_like(shard, identity):
    return jax.tree.map(
        lambda a, e: jnp.broadcast_to(jnp.asarray(e, a.dtype), a.shape), shard, identity
    )


def entering(shard, axes, combine, identity):
    before = start = neutral_like(shard, identity)
    subtotal = shard
    for axis in reversed(axes):
        devices, position = (lax.axis_size(axis), lax.axis_index(axis))
        pieces = jax.tree.map(lambda part: lax.all_gather(part, axis), subtotal)
        inside, subtotal = (start, start)
        for k in range(devices):
            passed = k < position
            subtotal = combine(subtotal, jax.tree.map(lambda part: part[k], pieces))
            inside = jax.tree.map(lambda new, old: jnp.where(passed, new, old), subtotal, inside)
        before = combine(inside, before)
    return before


def cut_along(shard, dim, devices):
    dims = shard.shape
    pieces = shard.reshape(*dims[:dim], devices, dims[dim] // devices, *dims[dim + 1 :])
    return jnp.moveaxis(pieces, dim, 0)


def summed_on_arrival(shard, axis, dim):
    pieces = cut_along(shard, dim, lax.axis_size(axis))
    arrived = lax.all_to_all(pieces, axis, split_axis=0, concat_axis=0, tiled=True)
    return arrived.astype(jnp.float32).sum(axis=0)


def rms_rows(rows, gain):
    values = rows.astype(jnp.float32)
    factor = lax.rsqrt(jnp.mean(values * values, axis=-1, keepdims=True) + epsilon)
    return (values * factor * gain.astype(jnp.float32)).astype(jnp.bfloat16)


def summary_join(earlier, latter):
    decay_first, peak_first, memory_first = earlier
    decay_second, peak_second, memory_second = latter
    peak_joined = jnp.maximum(decay_second + peak_first, peak_second)
    weight_first = jnp.exp(decay_second + peak_first - peak_joined)[..., None, None]
    weight_second = jnp.exp(peak_second - peak_joined)[..., None, None]
    return (
        decay_first + decay_second,
        peak_joined,
        weight_first * memory_first + weight_second * memory_second,
    )


def on_device(
    tokens,
    norm_gain,
    w_pool_in,
    w_mem_in,
    w_input_gate,
    w_forget_gate,
    forget_bias,
    forget_extra,
    conv_weight,
    query_map,
    key_map,
    pool_map,
    pool_gain,
    mem_gain,
    w_out_pool,
    w_out_mem,
):
    tp_index = lax.axis_index("tp")
    sp_index = lax.axis_index(SP)
    own_rows = tokens.shape[0]
    seq_rows = own_rows * lax.axis_size("tp")
    group_count = pool_map.shape[0]
    pool_cols = group_count * HEAD
    head_count = forget_extra.shape[1]
    mem_cols = head_count * HEAD
    blocks = seq_rows // BLOCK
    pool_enter, mem_enter, pool_leave, mem_leave = rows_first(
        (w_pool_in, w_mem_in, w_out_pool, w_out_mem), SP, (0, 0, 1, 1)
    )
    normalized = rms_rows(tokens, norm_gain)
    input_part = jnp.dot(normalized, w_input_gate, preferred_element_type=jnp.float32) * D ** (-0.5)
    forget_part = jnp.dot(normalized, w_forget_gate, preferred_element_type=jnp.float32)
    gate_rows = jnp.concatenate([input_part, forget_part], axis=1).astype(jnp.bfloat16)
    rows_all, gates_all = in_one_piece((normalized, gate_rows), "tp", 0, 1)
    pool_in = jnp.dot(rows_all, pool_enter, preferred_element_type=jnp.float32).astype(jnp.bfloat16)
    mem_in = jnp.dot(rows_all, mem_enter, preferred_element_type=jnp.float32).astype(jnp.bfloat16)
    head_start = tp_index * head_count
    input_pre = lax.dynamic_slice_in_dim(gates_all, head_start, head_count, 1).astype(jnp.float32)
    forget_pre = lax.dynamic_slice_in_dim(
        gates_all, MEMORY_HEADS + head_start, head_count, 1
    ).astype(jnp.float32)
    bias_own = lax.dynamic_slice_in_dim(forget_bias, head_start, head_count, 0)
    log_forget = jax.nn.log_sigmoid(forget_pre + bias_own) - forget_extra
    pool_rim, mem_rim = passed_along(
        (pool_in[seq_rows - 16 :], mem_in[seq_rows - (CONV - 1) :]), SP, 1
    )
    running = jnp.concatenate([pool_rim, pool_in], axis=0).astype(jnp.float32)
    stride_now = 1
    window_sums = []
    for window in windows_all:
        running = running[:-stride_now] + running[stride_now:]
        stride_now = window
        window_sums.append(running[17 - window : 17 - window + seq_rows])
    channel_group = tp_index * group_count + jnp.arange(pool_cols) // HEAD
    window_pick = channel_group % 4
    window_total = window_sums[0]
    for window_index in range(1, 4):
        window_total = jnp.where(
            window_pick == window_index, window_sums[window_index], window_total
        )
    window_len = (2 ** (window_pick + 1)).astype(jnp.float32)
    position = (sp_index * seq_rows + jnp.arange(seq_rows) + 1).astype(jnp.float32)
    counts = jnp.minimum(position[:, None], window_len[None, :])
    centred = (window_total / counts - pool_in.astype(jnp.float32)).astype(jnp.bfloat16)
    grouped = jnp.einsum(
        "tgc,gcd->tgd",
        centred.reshape(seq_rows, group_count, HEAD),
        pool_map,
        preferred_element_type=jnp.float32,
    )
    gain_own = lax.dynamic_slice_in_dim(pool_gain, tp_index * pool_cols, pool_cols, 0).astype(
        jnp.float32
    )
    pool_mixed = (grouped.reshape(seq_rows, pool_cols) * gain_own).astype(jnp.bfloat16)
    mem_ext = jnp.concatenate([mem_rim, mem_in], axis=0).astype(jnp.float32)
    conv_own = lax.dynamic_slice_in_dim(conv_weight, tp_index * mem_cols, mem_cols, 1).astype(
        jnp.float32
    )
    conv_sum = mem_ext[0:seq_rows] * conv_own[0]
    for tap_index in range(1, CONV):
        conv_sum = conv_sum + mem_ext[tap_index : tap_index + seq_rows] * conv_own[tap_index]
    conv_in = jax.nn.silu(conv_sum).astype(jnp.bfloat16)

    def dense_map(map_table):
        own_blocks = lax.dynamic_slice_in_dim(
            map_table, tp_index * (mem_cols // 4), mem_cols // 4, 0
        )
        own_blocks = own_blocks.astype(jnp.float32).reshape(head_count, HEAD // 4, 4, 4)
        spread = jnp.einsum("hbcd,be->hbced", own_blocks, jnp.eye(HEAD // 4, dtype=jnp.float32))
        return spread.reshape(head_count, HEAD, HEAD).astype(jnp.bfloat16)

    conv_heads = conv_in.reshape(seq_rows, head_count, HEAD)
    query_rows = jnp.einsum(
        "thc,hcd->thd", conv_heads, dense_map(query_map), preferred_element_type=jnp.float32
    ).astype(jnp.bfloat16)
    key_rows = jnp.einsum(
        "thc,hcd->thd", conv_heads, dense_map(key_map), preferred_element_type=jnp.float32
    ).astype(jnp.bfloat16)
    query_blocks = query_rows.reshape(blocks, BLOCK, head_count, HEAD)
    key_blocks = key_rows.reshape(blocks, BLOCK, head_count, HEAD)
    value_blocks = mem_in.reshape(blocks, BLOCK, head_count, HEAD)
    forget_blocks = jnp.swapaxes(log_forget.reshape(blocks, BLOCK, head_count), 1, 2)
    input_blocks = jnp.swapaxes(input_pre.reshape(blocks, BLOCK, head_count), 1, 2)
    cumulative = jnp.cumsum(forget_blocks, axis=-1)
    block_total = cumulative[..., -1]
    along_log = block_total[..., None] - cumulative + input_blocks
    along_peak = jnp.max(along_log, axis=-1)
    key_weight = jnp.exp(along_log - along_peak[..., None]) * HEAD ** (-0.5)
    scaled_keys = key_blocks.astype(jnp.float32) * jnp.swapaxes(key_weight, 1, 2)[..., None]
    block_memory = jnp.einsum(
        "nlhd,nlhe->nhde", scaled_keys, value_blocks.astype(jnp.float32), precision=highest
    )
    identity = (
        jnp.zeros((head_count,), jnp.float32),
        jnp.full((head_count,), lowest, jnp.float32),
        jnp.zeros((head_count, HEAD, HEAD), jnp.float32),
    )

    def local_step(summary, block_part):
        return (summary_join(summary, block_part), summary)

    device_summary, prefixes = lax.scan(
        local_step, identity, (block_total, along_peak, block_memory)
    )
    device_decay, device_peak, device_memory = device_summary
    incoming = entering((device_decay, device_peak, device_memory), SP, summary_join, identity)
    incoming_decay, incoming_peak, incoming_memory = incoming
    start_peak = jnp.maximum(incoming_decay, incoming_peak)
    start_memory = jnp.exp(incoming_peak - start_peak)[..., None, None] * incoming_memory
    unused_decay, block_peak, block_state = summary_join(
        (jnp.zeros((head_count,), jnp.float32), start_peak, start_memory), prefixes
    )
    causal_mask = jnp.tril(jnp.ones((BLOCK, BLOCK), dtype=jnp.bool_))
    log_diff = jnp.where(
        causal_mask,
        cumulative[..., :, None] - cumulative[..., None, :] + input_blocks[..., None, :],
        -jnp.inf,
    )
    carry_log = cumulative + block_peak[..., None]
    row_peak = jnp.maximum(jnp.max(log_diff, axis=-1), carry_log)
    scores = jnp.einsum(
        "nlhd,nshd->nhls", query_blocks, key_blocks, preferred_element_type=jnp.float32
    ) * HEAD ** (-0.5)
    block_weights = (jnp.exp(log_diff - row_peak[..., None]) * scores).astype(jnp.bfloat16)
    within_block = jnp.einsum(
        "nhls,nshe->nlhe", block_weights, value_blocks, preferred_element_type=jnp.float32
    )
    carried = jnp.einsum(
        "nlhd,nhde->nlhe", query_blocks.astype(jnp.float32), block_state, precision=highest
    )
    carried = carried * jnp.swapaxes(jnp.exp(carry_log - row_peak), 1, 2)[..., None]
    hidden = (within_block + carried).reshape(seq_rows, head_count, HEAD)
    centre = jnp.mean(hidden, axis=-1, keepdims=True)
    spread_sq = jnp.mean(jnp.square(hidden - centre), axis=-1, keepdims=True)
    normed = ((hidden - centre) * lax.rsqrt(spread_sq + epsilon)).reshape(seq_rows, mem_cols)
    mem_gain_own = lax.dynamic_slice_in_dim(mem_gain, tp_index * mem_cols, mem_cols, 0).astype(
        jnp.float32
    )
    mem_mixed = (normed * mem_gain_own).astype(jnp.bfloat16)
    summed = summed_on_arrival(
        (
            jnp.dot(pool_mixed, pool_leave, preferred_element_type=jnp.float32)
            + jnp.dot(mem_mixed, mem_leave, preferred_element_type=jnp.float32)
        ).astype(jnp.bfloat16),
        "tp",
        0,
    )
    return summed.astype(jnp.bfloat16)


def solution(mesh):
    torus = Mesh(mesh.devices.reshape(4, 4, mesh.shape["tp"]), ("sp_0", "sp_1", "tp"))
    in_specs = (
        P(SP_TP, None),
        P(),
        P(SP, "tp"),
        P(SP, "tp"),
        P(),
        P(),
        P(),
        P(SP, "tp"),
        P(),
        P(),
        P(),
        P("tp", None, None),
        P(),
        P(),
        P("tp", SP),
        P("tp", SP),
    )
    out_specs = P(SP_TP, None)
    return jax.shard_map(
        on_device, mesh=torus, in_specs=in_specs, out_specs=out_specs, check_vma=False
    )
```

profile of v0, /device:TPU:1, one launch (start us, length us, event | category | flops | bytes accessed | tf_op | source)
XLA Modules:
  0.0 330.2 jit_solution(7433710073949216774)
XLA Ops:
  6.6 0.8 convert_element_type.112
  7.4 1.2 fusion.47
  8.6 1.2 fusion.49
  9.7 1.1 fusion.46
  11.0 1.1 convolution_convert_fusion.2
  12.2 0.9 concatenate.15
  13.5 1.0 pad_maximum_fusion
  14.7 0.7 dynamic-slice_convert_fusion.1
  15.9 7.8 %fusion.9 = (bf16[2,64,4,64,4]{4,3,2,1,0:T(8,128)(2,1)}, bf16[2,64,4,64,4]{4,3,2,1,0:T(8,128)(2,1)}) fusion(f32[64,2,4,4]{3,2,0,1:T(4,128)S(1)} %copy.147, f32[64,64]{1,0:T(8,128)S(1)} %fusion.104, f32[64,2,4,4]{3,2,0,1:T(4,128)S(1)} %copy.138), kind=kLoop, calls=%fused_computation.19 | loop fusion | flops 524288 | bytes 557056 | tf_op jit(solution)/shard_map/convert_element_type | solution.py:188
  23.7 16.6 %convert_element_type.126 = bf16[2,256,256]{2,1,0:T(8,128)(2,1)S(1)} reshape(bf16[2,64,4,64,4]{4,3,2,1,0:T(8,128)(2,1)} %get-tuple-element.196) | data formatting | bytes 524288 | tf_op jit(solution)/shard_map/convert_element_type | solution.py:188
  40.4 17.2 %convert_element_type.135 = bf16[2,256,256]{2,1,0:T(8,128)(2,1)} reshape(bf16[2,64,4,64,4]{4,3,2,1,0:T(8,128)(2,1)} %get-tuple-element.195) | data formatting | bytes 524288 | tf_op jit(solution)/shard_map/convert_element_type | solution.py:188
  57.7 0.6 dynamic-slice
  58.8 0.6 broadcast_compare_fusion
  59.4 0.6 fusion.116
  60.1 0.6 add_convert_fusion.1
  60.7 1.4 dynamic-slice_convert_fusion.4
  62.0 0.7 dynamic-slice_convert_fusion.2
  62.7 0.6 iota_compare_fusion
  63.4 0.9 split.9
  64.6 0.9 reduce_window_sum.11
  66.1 99.1 %all-gather.12.cloned.1.call-done = bf16[4096,2048]{0,1:T(8,128)(2,1)} async-done(((bf16[256,2048]{0,1:T(8,128)(2,1)}), bf16[4096,2048]{0,1:T(8,128)(2,1)}) %all-gather.12.cloned.1.call-update) | async-done | bytes 16777232 | tf_op jit(solution)/shard_map/all_gather | solution.py:23
  165.2 5.0 %fusion.37 = bf16[384,512]{1,0:T(8,128)(2,1)S(1)} fusion(bf16[4096,2048]{0,1:T(8,128)(2,1)} %all-gather.12.cloned.1.call-done, bf16[384,4128]{1,0:T(8,128)(2,1)} %all-gather.10.cloned.1.call-done), kind=kOutput, calls=%fused_computation.41 | convolution fusion | flops 1610809344 | bytes 7733248 | tf_op jit(solution)/shard_map/dot_general | solution.py:134
  170.2 2.8 collective-permute-start.1
  173.2 0.7 copy.153
  174.0 0.5 multiply_convert_fusion.3
  175.0 0.9 fusion.58
  176.0 16.5 %while.21 = (s32[]{:T(128)}, f32[2]{0:T(128)}, f32[2]{0:T(128)S(1)}, f32[2,256,256]{2,1,0:T(8,128)S(1)}, f32[3,2]{1,0:T(4,128)}, /*index=5*/f32[3,2]{1,0:T(4,128...) while((s32[]{:T(128)}, f32[2]{0:T(128)}, ...), condition=%wide.region_5.6_spmd.clone, body=%wide.region_4.5_spmd.clone.sunk | while | flops 655377 | bytes 2622245 | solution.py:220
  176.0 1.3 subtract_exponential_fusion.19
  177.3 0.7 subtract_exponential_fusion.20
  178.0 0.9 bitcast_dynamic-update-slice_fusion.2
  179.0 1.3 dynamic_update_slice.19
  180.2 1.3 dynamic_update_slice.20
  181.5 1.3 subtract_exponential_fusion.19
  182.8 0.7 subtract_exponential_fusion.20
  183.5 0.8 bitcast_dynamic-update-slice_fusion.2
  184.4 1.3 dynamic_update_slice.19
  185.7 1.3 dynamic_update_slice.20
  187.0 1.3 subtract_exponential_fusion.19
  188.2 0.7 subtract_exponential_fusion.20
  188.9 0.9 bitcast_dynamic-update-slice_fusion.2
  189.9 1.3 dynamic_update_slice.19
  191.2 1.3 dynamic_update_slice.20
  192.5 0.8 copy-done.1
  193.6 1.1 fusion.91
  194.7 5.0 %fusion.32 = bf16[384,512]{1,0:T(8,128)(2,1)S(1)} fusion(bf16[4096,2048]{0,1:T(8,128)(2,1)} %all-gather.12.cloned.1.call-done, bf16[384,4128]{1,0:T(8,128)(2,1)} %all-gather.10.cloned.1.call-done), kind=kOutput, calls=%fused_computation.40 | convolution fusion | flops 1610809344 | bytes 7733248 | tf_op jit(solution)/shard_map/dot_general | solution.py:133
  200.2 3.4 %collective-permute-start = (bf16[16,512]{1,0:T(8,128)(2,1)S(1)}, bf16[16,512]{1,0:T(8,128)(2,1)S(1)}, u32[]{:S(2)}, u32[]{:S(2)}) collective-permute-start(bf16[16,512]{1,0:T(8,128)(2,1)S(1)} %slice.225), channel_id=1, source_target_pairs={{0,8},{8,16},{16,24},{24,32},{32,40},{40,48},{48,56},{56,64},{64,7... | collective-permute-start | bytes 49160 | tf_op jit(solution)/shard_map/ppermute | solution.py:43
  203.6 11.7 %all-reduce.2 = (f32[8]{0:T(128)S(1)}, f32[8]{0:T(128)S(1)}) all-reduce(f32[8]{0:T(128)S(1)} %dynamic-update-slice.1, f32[8]{0:T(128)S(1)} %dynamic-update-slice), channel_id=3, replica_groups=mesh['sp_0'=4,'sp_1'=4,'tp'=8] {'sp_1'}, use_global_device_ids=true, to_apply=%add.1 | all-reduce | flops 16 | bytes 128
  215.4 6.0 %all-gather.3 = f32[4,1,2]{2,1,0:T(1,128)S(1)} all-gather(f32[1,1,2]{2,1,0:T(1,128)S(1)} %get-tuple-element.225), channel_id=1, replica_groups=mesh['sp_0'=4,'sp_1'=4,'tp'=8] {'sp_0'}, dimensions={0}, use_global_device_ids=true | all-gather | bytes 40 | tf_op jit(solution)/shard_map/all_gather | solution.py:57
  221.4 7.1 %all-gather.4 = f32[4,1,2]{2,1,0:T(1,128)S(1)} all-gather(f32[1,1,2]{2,1,0:T(1,128)S(1)} %get-tuple-element.186), channel_id=1, replica_groups=mesh['sp_0'=4,'sp_1'=4,'tp'=8] {'sp_0'}, dimensions={0}, use_global_device_ids=true | all-gather | bytes 40 | tf_op jit(solution)/shard_map/all_gather | solution.py:57
  229.2 0.6 fusion.118
  229.8 0.6 subtract_exponential_fusion.15
  230.7 2.6 fusion.74
  233.3 1.4 convolution_bitcast_fusion
  234.7 0.6 subtract_exponential_fusion.16
  236.4 0.5 fusion.63
  237.5 6.8 %fusion.13 = f32[384,4096]{1,0:T(8,128)} fusion(bf16[384,512]{0,1:T(8,128)(2,1)S(1)} %fusion.57, bf16[4096,2048]{0,1:T(8,128)(2,1)} %all-gather.12.cloned.1.call-done), kind=kOutput, calls=%fused_computation.24 | convolution fusion | flops 1610612736 | bytes 10878976 | tf_op jit(solution)/shard_map/dot_general | solution.py:260
  244.3 23.6 %all-gather.14.cloned.1.call-done = f32[4,2,256,256]{3,2,1,0:T(8,128)} async-done(((f32[1,2,256,256]{3,2,1,0:T(8,128)}), f32[4,2,256,256]{3,2,1,0:T(8,128)}) %all-gather.14.cloned.1.call-update) | async-done | bytes 2097168 | tf_op jit(solution)/shard_map/all_gather | solution.py:57
  267.9 2.4 fusion.69
  270.3 1.6 fusion.141
  271.9 0.6 copy.156
  272.8 0.5 mul.511
  274.1 5.9 %add_convert_fusion = bf16[384,4096]{1,0:T(8,128)(2,1)S(1)} fusion(f32[384,4096]{1,0:T(8,128)} %fusion.13, bf16[4096,2048]{0,1:T(8,128)(2,1)} %all-gather.12.cloned.1.call-done, f32[384,512]{1,0:T(8,128)S(1)} %bitcast.394, f32[384,512]{1,0:T(8,128)S(1)} %bitcast.396, f32[384,512]{1,0:T(8,128)S(1)} %bitcast.395, f32[512]{0:T(512)S(1)} %copy-done.15), kind=kOutput, calls=%fused_computation.20 | convolution fusion | flops 1614544896 | bytes 15992832 | tf_op jit(solution)/shard_map/dot_general | solution.py:261
  280.1 42.3 %all_to_all.5 = bf16[8,48,4096]{2,1,0:T(8,128)(2,1)S(1)} all-to-all(bf16[8,48,4096]{2,1,0:T(8,128)(2,1)S(1)} %bitcast.393), channel_id=1, replica_groups=mesh['sp_0'=4,'sp_1'=4,'tp'=8] {'tp'}, dimensions={0} | all-to-all | bytes 6291456 | tf_op jit(solution)/shard_map/all_to_all | solution.py:75
  322.4 1.3 reduce_sum.42
  (152 shorter events, 7.6 us)
Async XLA Ops:
  6.5 230.4 %copy-start = (bf16[2,256,256]{2,1,0:T(8,128)(2,1)S(1)}, bf16[2,256,256]{2,1,0:T(8,128)(2,1)}, u32[]{:S(2)}) copy-start(bf16[2,256,256]{2,1,0:T(8,128)(2,1)} %param.29) | copy-start | bytes 786436
  6.5 6.6 %copy-start.6 = (bf16[256,512]{1,0:T(8,128)(2,1)S(1)}, bf16[256,512]{1,0:T(8,128)(2,1)}, u32[]{:S(2)}) copy-start(bf16[256,512]{1,0:T(8,128)(2,1)} %param.20) | copy-start | bytes 786436
  6.5 6.8 %copy-start.7 = (bf16[256,512]{1,0:T(8,128)(2,1)S(1)}, bf16[256,512]{1,0:T(8,128)(2,1)}, u32[]{:S(2)}) copy-start(bf16[256,512]{1,0:T(8,128)(2,1)} %param.21) | copy-start | bytes 786436
  6.5 6.9 %copy-start.9 = (bf16[512,256]{1,0:T(8,128)(2,1)S(1)}, bf16[512,256]{1,0:T(8,128)(2,1)}, u32[]{:S(2)}) copy-start(bf16[512,256]{1,0:T(8,128)(2,1)} %param.32) | copy-start | bytes 786436
  6.5 6.9 %copy-start.8 = (bf16[512,256]{1,0:T(8,128)(2,1)S(1)}, bf16[512,256]{1,0:T(8,128)(2,1)}, u32[]{:S(2)}) copy-start(bf16[512,256]{1,0:T(8,128)(2,1)} %param.33) | copy-start | bytes 786436
  6.5 56.8 %all-gather.10.cloned.1.call-start = ((), (), s32[]{:S(2)}) async-start(), calls=%async_computation.1 | async-start | bytes 3649536 | tf_op jit(solution)/shard_map/all_gather | solution.py:37
  13.1 152.1 %all-gather.12.cloned.1.call-start = ((), (), s32[]{:S(2)}) async-start(), calls=%async_computation.2 | async-start | bytes 17825792 | tf_op jit(solution)/shard_map/all_gather | solution.py:23
  14.5 216.2 %all-gather.16.cloned.1.call-start = ((), (), s32[]{:S(2)}) async-start(), calls=%async_computation.4 | async-start | bytes 2621440 | tf_op jit(solution)/shard_map/all_gather | solution.py:57
  40.3 17.3 %copy-start.34 = (f32[16]{0:T(128)S(1)}, f32[16]{0:T(128)}, u32[]{:S(2)}) copy-start(f32[16]{0:T(128)} %param.24) | copy-start | bytes 196
  40.4 17.3 %copy-start.35 = (u32[128]{0:T(128)S(1)}, u32[128]{0:T(128)}, u32[]{:S(2)}) copy-start(u32[128]{0:T(128)} %constant.147) | copy-start | bytes 1540
  40.4 24.1 %copy-start.30 = (f32[384,2]{0,1:T(2,128)S(1)}, f32[384,2]{0,1:T(2,128)}, u32[]{:S(2)}) copy-start(f32[384,2]{0,1:T(2,128)} %param.25) | copy-start | bytes 9220
  65.8 107.2 %copy-start.14 = (f32[3,2]{1,0:T(4,128)}, f32[3,2]{1,0:T(4,128)S(1)}, u32[]{:S(2)}) copy-start(f32[3,2]{1,0:T(4,128)S(1)} %copy.146) | copy-start | bytes 76
  65.9 107.1 %copy-start.11 = (f32[384,2]{0,1:T(2,128)}, f32[384,2]{0,1:T(2,128)S(1)}, u32[]{:S(2)}) copy-start(f32[384,2]{0,1:T(2,128)S(1)} %copy.173) | copy-start | bytes 9220
  66.1 106.9 %copy-start.13 = (f32[3,2]{1,0:T(4,128)}, f32[3,2]{1,0:T(4,128)S(1)}, u32[]{:S(2)}) copy-start(f32[3,2]{1,0:T(4,128)S(1)} %add_reduce_fusion) | copy-start | bytes 76
  170.2 3.7 %collective-permute-start.1 = (bf16[3,512]{1,0:T(4,128)(2,1)S(1)}, bf16[3,512]{1,0:T(4,128)(2,1)S(1)}, u32[]{:S(2)}, u32[]{:S(2)}) collective-permute-start(bf16[3,512]{1,0:T(4,128)(2,1)S(1)} %slice.242), channel_id=1, source_target_pairs={{0,8},{8,16},{16,24},{24,32},{32,40},{40,48},{48,56},{56,64},{64,7... | collective-permute-start | bytes 9224 | tf_op jit(solution)/shard_map/ppermute | solution.py:43
  192.5 0.8 copy-start.1
  193.3 74.6 %all-gather.14.cloned.1.call-start = ((), (), s32[]{:S(2)}) async-start(), calls=%async_computation.3 | async-start | bytes 2621440 | tf_op jit(solution)/shard_map/all_gather | solution.py:57
  194.6 5.1 %copy-start.16 = (f32[2]{0:T(128)S(1)}, f32[2]{0:T(128)}, u32[]{:S(2)}) copy-start(f32[2]{0:T(128)} %get-tuple-element.63) | copy-start | bytes 28
  194.6 33.9 %copy-start.4 = (bf16[2,256,256]{2,1,0:T(8,128)(2,1)S(1)}, bf16[2,256,256]{2,1,0:T(8,128)(2,1)}, u32[]{:S(2)}) copy-start(bf16[2,256,256]{2,1,0:T(8,128)(2,1)} %convert_element_type.135) | copy-start | bytes 786436
  194.6 34.5 %copy-start.20 = (f32[3,2]{1,0:T(4,128)S(1)}, f32[3,2]{1,0:T(4,128)}, u32[]{:S(2)}) copy-start(f32[3,2]{1,0:T(4,128)} %get-tuple-element.65) | copy-start | bytes 76
  194.6 34.5 %copy-start.31 = (f32[3,2]{1,0:T(4,128)S(1)}, f32[3,2]{1,0:T(4,128)}, u32[]{:S(2)}) copy-start(f32[3,2]{1,0:T(4,128)} %get-tuple-element.62) | copy-start | bytes 76
  199.7 33.6 %copy-start.10 = (pred[128,128]{1,0:T(8,128)(4,1)S(1)}, pred[128,128]{1,0:T(8,128)(4,1)}, u32[]{:S(2)}) copy-start(pred[128,128]{1,0:T(8,128)(4,1)} %iota_compare_fusion) | copy-start | bytes 49156
  199.7 33.6 %copy-start.12 = (f32[384,2]{0,1:T(2,128)S(1)}, f32[384,2]{0,1:T(2,128)}, u32[]{:S(2)}) copy-start(f32[384,2]{0,1:T(2,128)} %copy-done.11) | copy-start | bytes 9220
  200.2 35.1 %collective-permute-start = (bf16[16,512]{1,0:T(8,128)(2,1)S(1)}, bf16[16,512]{1,0:T(8,128)(2,1)S(1)}, u32[]{:S(2)}, u32[]{:S(2)}) collective-permute-start(bf16[16,512]{1,0:T(8,128)(2,1)S(1)} %slice.225), channel_id=1, source_target_pairs={{0,8},{8,16},{16,24},{24,32},{32,40},{40,48},{48,56},{56,64},{64,7... | collective-permute-start | bytes 49160 | tf_op jit(solution)/shard_map/ppermute | solution.py:43
  230.5 4.9 %copy-start.21 = (f32[2]{0:T(128)}, f32[2]{0:T(128)S(1)}, u32[]{:S(2)}) copy-start(f32[2]{0:T(128)S(1)} %get-tuple-element.215) | copy-start | bytes 28
  230.5 4.9 %copy-start.23 = (f32[2]{0:T(128)}, f32[2]{0:T(128)S(1)}, u32[]{:S(2)}) copy-start(f32[2]{0:T(128)S(1)} %get-tuple-element.216) | copy-start | bytes 28
  230.5 4.9 %copy-start.24 = (f32[2]{0:T(128)}, f32[2]{0:T(128)S(1)}, u32[]{:S(2)}) copy-start(f32[2]{0:T(128)S(1)} %get-tuple-element.217) | copy-start | bytes 28
  230.5 4.9 %copy-start.25 = (f32[2]{0:T(128)}, f32[2]{0:T(128)S(1)}, u32[]{:S(2)}) copy-start(f32[2]{0:T(128)S(1)} %get-tuple-element.218) | copy-start | bytes 28
  230.5 4.9 %copy-start.26 = (f32[2]{0:T(128)}, f32[2]{0:T(128)S(1)}, u32[]{:S(2)}) copy-start(f32[2]{0:T(128)S(1)} %get-tuple-element.219) | copy-start | bytes 28
  230.5 4.9 %copy-start.27 = (f32[2]{0:T(128)}, f32[2]{0:T(128)S(1)}, u32[]{:S(2)}) copy-start(f32[2]{0:T(128)S(1)} %get-tuple-element.220) | copy-start | bytes 28
  230.5 4.9 %copy-start.28 = (f32[2]{0:T(128)}, f32[2]{0:T(128)S(1)}, u32[]{:S(2)}) copy-start(f32[2]{0:T(128)S(1)} %get-tuple-element.221) | copy-start | bytes 28
  230.5 4.9 %copy-start.29 = (f32[2]{0:T(128)}, f32[2]{0:T(128)S(1)}, u32[]{:S(2)}) copy-start(f32[2]{0:T(128)S(1)} %get-tuple-element.222) | copy-start | bytes 28
  235.7 0.7 copy-start.17
  235.7 0.7 copy-start.18
  235.7 0.7 copy-start.32
  235.7 0.7 copy-start.33
  236.1 1.2 copy-start.19
  237.5 30.4 %copy-start.2 = (f32[8,256,256]{2,1,0:T(8,128)S(1)}, f32[8,256,256]{2,1,0:T(8,128)}, u32[]{:S(2)}) copy-start(f32[8,256,256]{2,1,0:T(8,128)} %all-gather.16.cloned.1.call-done) | copy-start | bytes 6291460
  237.5 30.4 %copy-start.22 = (f32[2]{0:T(128)S(1)}, f32[2]{0:T(128)}, u32[]{:S(2)}) copy-start(f32[2]{0:T(128)} %copy-done.21) | copy-start | bytes 28
  244.3 26.0 %copy-start.5 = (f32[3,128,2,256]{1,3,2,0:T(8,128)S(1)}, f32[3,128,2,256]{1,3,2,0:T(8,128)}, u32[]{:S(2)}) copy-start(f32[3,128,2,256]{1,3,2,0:T(8,128)} %convolution_bitcast_fusion) | copy-start | bytes 2359300
  267.9 2.4 copy-start.3
  273.3 0.8 copy-start.15
Sparse Core Ops, SparseCore 0:
  13.2 31.6 all-gather.9
  47.0 118.1 all-gather.11
  193.4 34.3 all-gather.15
  233.4 34.4 all-gather.13
where the time goes:
time: 331 us; the launch traced here: 330 us
  waiting for transfers between devices  123 us (37%)
  blocking collectives  67.1 us (20%)
  local copies, waits for them, and re-layouts  50.4 us (15%)
  other arithmetic  38.8 us (12%)
  matrix products  29.9 us (9%)
  between operations  14.6 us (4%)
  starting transfers between devices  6.58 us (2%)
    all_gather x1, waiting for transfers between devices, rows_first(): lax.all_gather(both, axis, axis=0, tiled=True)  99.1 us
    all_to_all x1, blocking collectives, summed_on_arrival(): lax.all_to_all(pieces, axis, split_axis=0, concat_axis=0, tiled=True)  42.3 us
    convert_element_type x2, local copies, waits for them, and re-layouts, dense_map(): return spread.reshape(head_count, HEAD, HEAD).astype(jnp.bfloat16)  33.8 us
    all_gather x2, waiting for transfers between devices, entering(): pieces = jax.tree.map(lambda part: lax.all_gather(part, axis), subtotal)  23.6 us
    all_gather x2, blocking collectives, entering(): pieces = jax.tree.map(lambda part: lax.all_gather(part, axis), subtotal)  13.1 us
    unnamed x1, blocking collectives  11.7 us
    convert_element_type x1, other arithmetic, dense_map(): return spread.reshape(head_count, HEAD, HEAD).astype(jnp.bfloat16)  7.81 us
    dynamic_update_slice x6, local copies, waits for them, and re-layouts, on_device(): lax.scan(local_step, identity, (block_total, along_peak, block_memory))  7.64 us
  transfers between devices with their start and end apart: 6, of which 2 were waited for; matrix products, arithmetic and copies ran while one was open for 23% of the time, Pallas kernels for 0%

commit v1 on v0

--- a/solution.py
+++ b/solution.py
@@ -20,7 +20,13 @@
 def rows_first(arrays, axis, dims):
     turned = [jnp.moveaxis(a, dim, 0) for a, dim in zip(arrays, dims)]
     both = jnp.concatenate([t.reshape(len(t), -1) for t in turned], axis=1)
-    filled, at, gathered = (lax.all_gather(both, axis, axis=0, tiled=True), 0, [])
+    filled, at, gathered = (
+        jnp.concatenate(
+            lax.all_to_all(jnp.stack([both] * lax.axis_size(axis)), axis, 0, 0), axis=0
+        ),
+        0,
+        [],
+    )
     for t, dim in zip(turned, dims):
         piece = filled[:, at : at + t[0].size].reshape(-1, *t.shape[1:])
         gathered.append(jnp.moveaxis(piece, 0, dim))

time: 331 us -> 440 us (1.33)
  waiting for transfers between devices: 123 us -> 220 us
  local copies, waits for them, and re-layouts: 50.4 us -> 59.1 us
  starting transfers between devices: 6.58 us -> 13.8 us
    all_to_all x0 -> x1, waiting for transfers between devices: none -> 196 us  [rows_first(): lax.all_to_all(jnp.stack([both] * lax.axis_size(axis)), axis, 0, 0)]
    all_gather x1 -> x0, waiting for transfers between devices: 99.1 us -> none  [rows_first(): lax.all_gather(both, axis, axis=0, tiled=True)]
    all_to_all x0 -> x1, starting transfers between devices: none -> 8.78 us  [rows_first(): lax.all_to_all(jnp.stack([both] * lax.axis_size(axis)), axis, 0, 0)]
    another operation x6 -> x7, local copies, waits for them, and re-layouts: 0.72 us -> 6.74 us  [the longest x1 6.02 us: rows_first(): jnp.stack([both] * lax.axis_size(axis))]
  transfers between devices with their start and end apart: 6 -> 6, of which waited for: 2 -> 2; matrix products, arithmetic and copies ran while one was open for 23% -> 17% of each run, Pallas kernels for 0% -> 0%
where the time goes in v1:
time: 440 us; the launch traced here: 439 us
  waiting for transfers between devices  220 us (50%)
  blocking collectives  67.2 us (15%)
  local copies, waits for them, and re-layouts  59.1 us (13%)
  other arithmetic  36 us (8%)
  matrix products  28 us (6%)
  between operations  14.6 us (3%)
  starting transfers between devices  13.8 us (3%)
    all_to_all x1, waiting for transfers between devices, rows_first(): lax.all_to_all(jnp.stack([both] * lax.axis_size(axis)), axis, 0, 0)  196 us
    all_to_all x1, blocking collectives, summed_on_arrival(): lax.all_to_all(pieces, axis, split_axis=0, concat_axis=0, tiled=True)  42.3 us
    convert_element_type x2, local copies, waits for them, and re-layouts, dense_map(): return spread.reshape(head_count, HEAD, HEAD).astype(jnp.bfloat16)  33.8 us
    all_gather x2, waiting for transfers between devices, entering(): pieces = jax.tree.map(lambda part: lax.all_gather(part, axis), subtotal)  24.2 us
    all_gather x2, blocking collectives, entering(): pieces = jax.tree.map(lambda part: lax.all_gather(part, axis), subtotal)  14.3 us
    unnamed x1, blocking collectives  10.5 us
  transfers between devices with their start and end apart: 6, of which 2 were waited for; matrix products, arithmetic and copies ran while one was open for 17% of the time, Pallas kernels for 0%

profile of v1, /device:TPU:1, one launch (start us, length us, event | category | flops | bytes accessed | tf_op | source)
XLA Modules:
  0.0 438.7 jit_solution(4118447603560286749)
XLA Ops:
  6.5 1.1 copy.133
  7.7 1.1 copy.134
  8.8 1.1 pad_maximum_fusion
  9.9 0.6 copy.135
  10.5 6.0 %stack.2 = bf16[16,256,2048]{2,1,0:T(8,128)(2,1)} broadcast(bf16[256,2048]{1,0:T(8,128)(2,1)S(1)} %copy.135), dimensions={1,2} | broadcast | bytes 17825792 | tf_op jit(solution)/shard_map/stack | solution.py:25
  16.6 8.8 %all-to-all-start = ((bf16[16,256,2048]{2,1,0:T(8,128)(2,1)}), bf16[16,256,2048]{2,1,0:T(8,128)(2,1)}, u32[]{:S(2)}, u32[]{:S(2)}) async-start(bf16[16,256,2048]{2,1,0:T(8,128)(2,1)} %stack.2), calls=%async_computation | async-start | bytes 33554432 | tf_op jit(solution)/shard_map/all_to_all | solution.py:25
  26.4 0.9 concatenate.15
  27.5 0.7 dynamic-slice_convert_fusion.1
  28.7 7.8 %fusion.9 = (bf16[2,64,4,64,4]{4,3,2,1,0:T(8,128)(2,1)}, bf16[2,64,4,64,4]{4,3,2,1,0:T(8,128)(2,1)}) fusion(f32[64,2,4,4]{3,2,0,1:T(4,128)S(1)} %copy.152, f32[64,64]{1,0:T(8,128)S(1)} %fusion.104, f32[64,2,4,4]{3,2,0,1:T(4,128)S(1)} %copy.143), kind=kLoop, calls=%fused_computation.19 | loop fusion | flops 524288 | bytes 557056 | tf_op jit(solution)/shard_map/convert_element_type | solution.py:194
  36.5 16.6 %convert_element_type.126 = bf16[2,256,256]{2,1,0:T(8,128)(2,1)S(1)} reshape(bf16[2,64,4,64,4]{4,3,2,1,0:T(8,128)(2,1)} %get-tuple-element.196) | data formatting | bytes 524288 | tf_op jit(solution)/shard_map/convert_element_type | solution.py:194
  53.2 17.3 %convert_element_type.135 = bf16[2,256,256]{2,1,0:T(8,128)(2,1)} reshape(bf16[2,64,4,64,4]{4,3,2,1,0:T(8,128)(2,1)} %get-tuple-element.195) | data formatting | bytes 524288 | tf_op jit(solution)/shard_map/convert_element_type | solution.py:194
  70.5 0.6 dynamic-slice
  71.7 0.6 broadcast_compare_fusion
  72.2 0.6 fusion.116
  72.9 0.6 add_convert_fusion.1
  73.5 1.4 dynamic-slice_convert_fusion.4
  74.8 0.7 dynamic-slice_convert_fusion.2
  75.5 0.6 iota_compare_fusion
  76.2 0.9 split.9
  77.4 0.9 reduce_window_sum.11
  78.9 195.6 %all-to-all-done = bf16[16,256,2048]{2,1,0:T(8,128)(2,1)} async-done(((bf16[16,256,2048]{2,1,0:T(8,128)(2,1)}), bf16[16,256,2048]{2,1,0:T(8,128)(2,1)}, u32[]{:S(2)}, u32[]{:S(2)}) %all-to-all-start) | async-done | bytes 16777248 | tf_op jit(solution)/shard_map/all_to_all | solution.py:25
  274.5 4.9 %fusion.37 = bf16[384,512]{1,0:T(8,128)(2,1)S(1)} fusion(bf16[4096,2048]{1,0:T(8,128)(2,1)} %bitcast.2, bf16[384,4128]{1,0:T(8,128)(2,1)} %all-gather.9.cloned.1.call-done), kind=kOutput, calls=%fused_computation.41 | convolution fusion | flops 1610809344 | bytes 7733248 | tf_op jit(solution)/shard_map/dot_general | solution.py:140
  279.4 1.3 collective-permute-start.1
  280.9 0.7 copy.158
  281.7 0.5 multiply_convert_fusion.3
  282.8 0.9 fusion.58
  283.7 16.6 %while.21 = (s32[]{:T(128)}, f32[2]{0:T(128)}, f32[2]{0:T(128)S(1)}, f32[2,256,256]{2,1,0:T(8,128)S(1)}, f32[3,2]{1,0:T(4,128)}, /*index=5*/f32[3,2]{1,0:T(4,128...) while((s32[]{:T(128)}, f32[2]{0:T(128)}, ...), condition=%wide.region_5.6_spmd.clone, body=%wide.region_4.5_spmd.clone.sunk | while | flops 655377 | bytes 2622245 | solution.py:226
  283.7 1.3 subtract_exponential_fusion.19
  285.0 0.7 subtract_exponential_fusion.20
  285.7 0.9 bitcast_dynamic-update-slice_fusion.2
  286.7 1.3 dynamic_update_slice.19
  288.0 1.3 dynamic_update_slice.20
  289.3 1.3 subtract_exponential_fusion.19
  290.5 0.7 subtract_exponential_fusion.20
  291.2 0.8 bitcast_dynamic-update-slice_fusion.2
  292.2 1.3 dynamic_update_slice.19
  293.5 1.3 dynamic_update_slice.20
  294.8 1.3 subtract_exponential_fusion.19
  296.0 0.7 subtract_exponential_fusion.20
  296.7 0.9 bitcast_dynamic-update-slice_fusion.2
  297.7 1.3 dynamic_update_slice.19
  299.0 1.3 dynamic_update_slice.20
  300.3 0.8 copy-done.1
  301.4 1.1 fusion.91
  302.5 5.0 %fusion.32 = bf16[384,512]{1,0:T(8,128)(2,1)S(1)} fusion(bf16[4096,2048]{1,0:T(8,128)(2,1)} %bitcast.2, bf16[384,4128]{1,0:T(8,128)(2,1)} %all-gather.9.cloned.1.call-done), kind=kOutput, calls=%fused_computation.40 | convolution fusion | flops 1610809344 | bytes 7733248 | tf_op jit(solution)/shard_map/dot_general | solution.py:139
  307.9 3.4 collective-permute-start
  311.4 10.5 %all-reduce.2 = (f32[8]{0:T(128)S(1)}, f32[8]{0:T(128)S(1)}) all-reduce(f32[8]{0:T(128)S(1)} %dynamic-update-slice.1, f32[8]{0:T(128)S(1)} %dynamic-update-slice), channel_id=3, replica_groups=mesh['sp_0'=4,'sp_1'=4,'tp'=8] {'sp_1'}, use_global_device_ids=true, to_apply=%add.1 | all-reduce | flops 16 | bytes 128
  322.0 8.7 %all-gather.3 = f32[4,1,2]{2,1,0:T(1,128)S(1)} all-gather(f32[1,1,2]{2,1,0:T(1,128)S(1)} %get-tuple-element.225), channel_id=1, replica_groups=mesh['sp_0'=4,'sp_1'=4,'tp'=8] {'sp_0'}, dimensions={0}, use_global_device_ids=true | all-gather | bytes 40 | tf_op jit(solution)/shard_map/all_gather | solution.py:63
  330.7 5.6 %all-gather.4 = f32[4,1,2]{2,1,0:T(1,128)S(1)} all-gather(f32[1,1,2]{2,1,0:T(1,128)S(1)} %get-tuple-element.186), channel_id=1, replica_groups=mesh['sp_0'=4,'sp_1'=4,'tp'=8] {'sp_0'}, dimensions={0}, use_global_device_ids=true | all-gather | bytes 40 | tf_op jit(solution)/shard_map/all_gather | solution.py:63
  337.0 0.6 fusion.118
  337.6 0.6 subtract_exponential_fusion.15
  338.5 2.6 fusion.74
  341.1 1.4 convolution_bitcast_fusion
  342.5 0.6 subtract_exponential_fusion.16
  344.2 0.5 fusion.63
  345.3 6.9 %fusion.13 = f32[384,4096]{1,0:T(8,128)} fusion(bf16[384,512]{0,1:T(8,128)(2,1)S(1)} %fusion.57, bf16[4096,2048]{1,0:T(8,128)(2,1)} %bitcast.2), kind=kOutput, calls=%fused_computation.24 | convolution fusion | flops 1610612736 | bytes 10878976 | tf_op jit(solution)/shard_map/dot_general | solution.py:266
  352.1 24.2 %all-gather.11.cloned.1.call-done = f32[4,2,256,256]{3,2,1,0:T(8,128)} async-done(((f32[1,2,256,256]{3,2,1,0:T(8,128)}), f32[4,2,256,256]{3,2,1,0:T(8,128)}) %all-gather.11.cloned.1.call-update) | async-done | bytes 2097168 | tf_op jit(solution)/shard_map/all_gather | solution.py:63
  376.4 2.4 fusion.69
  378.8 1.6 fusion.141
  380.4 0.6 copy.161
  381.3 0.5 mul.511
  382.6 5.9 %add_convert_fusion = bf16[384,4096]{1,0:T(8,128)(2,1)S(1)} fusion(f32[384,4096]{1,0:T(8,128)} %fusion.13, bf16[4096,2048]{1,0:T(8,128)(2,1)} %bitcast.2, f32[384,512]{1,0:T(8,128)S(1)} %bitcast.397, f32[384,512]{1,0:T(8,128)S(1)} %bitcast.399, f32[384,512]{1,0:T(8,128)S(1)} %bitcast.398, f32[512]{0:T(512)S(1)} %copy-done.17), kind=kOutput, calls=%fused_computation.20 | convolution fusion | flops 1614544896 | bytes 15992832 | tf_op jit(solution)/shard_map/dot_general | solution.py:267
  388.5 42.3 %all_to_all.10 = bf16[8,48,4096]{2,1,0:T(8,128)(2,1)S(1)} all-to-all(bf16[8,48,4096]{2,1,0:T(8,128)(2,1)S(1)} %bitcast.394), channel_id=1, replica_groups=mesh['sp_0'=4,'sp_1'=4,'tp'=8] {'tp'}, dimensions={0} | all-to-all | bytes 6291456 | tf_op jit(solution)/shard_map/all_to_all | solution.py:81
  430.8 1.3 reduce_sum.42
  (153 shorter events, 8.0 us)
Async XLA Ops:
  6.5 338.2 %copy-start = (bf16[2,256,256]{2,1,0:T(8,128)(2,1)S(1)}, bf16[2,256,256]{2,1,0:T(8,128)(2,1)}, u32[]{:S(2)}) copy-start(bf16[2,256,256]{2,1,0:T(8,128)(2,1)} %param.29) | copy-start | bytes 786436
  16.5 8.9 %copy-start.19 = (bf16[4096]{0:T(1024)(128)(2,1)S(1)}, bf16[4096]{0:T(1024)(128)(2,1)}, u32[]{:S(2)}) copy-start(bf16[4096]{0:T(1024)(128)(2,1)} %param.19) | copy-start | bytes 24580
  16.5 8.9 %copy-start.4 = (bf16[48,4096]{1,0:T(8,128)(2,1)S(1)}, bf16[48,4096]{1,0:T(8,128)(2,1)}, u32[]{:S(2)}) copy-start(bf16[48,4096]{1,0:T(8,128)(2,1)} %param.18) | copy-start | bytes 1179652
  16.5 9.3 %copy-start.7 = (bf16[4096,16]{0,1:T(8,128)(2,1)S(1)}, bf16[4096,16]{0,1:T(8,128)(2,1)}, u32[]{:S(2)}) copy-start(bf16[4096,16]{0,1:T(8,128)(2,1)} %param.22) | copy-start | bytes 393220
  16.5 9.6 %copy-start.8 = (bf16[4096,16]{0,1:T(8,128)(2,1)S(1)}, bf16[4096,16]{0,1:T(8,128)(2,1)}, u32[]{:S(2)}) copy-start(bf16[4096,16]{0,1:T(8,128)(2,1)} %param.23) | copy-start | bytes 393220
  16.6 257.9 %all-to-all-start = ((bf16[16,256,2048]{2,1,0:T(8,128)(2,1)}), bf16[16,256,2048]{2,1,0:T(8,128)(2,1)}, u32[]{:S(2)}, u32[]{:S(2)}) async-start(bf16[16,256,2048]{2,1,0:T(8,128)(2,1)} %stack.2), calls=%async_computation | async-start | bytes 33554432 | tf_op jit(solution)/shard_map/all_to_all | solution.py:25
  25.3 50.8 %all-gather.9.cloned.1.call-start = ((), (), s32[]{:S(2)}) async-start(), calls=%async_computation.2 | async-start | bytes 3649536 | tf_op jit(solution)/shard_map/all_gather | solution.py:43
  27.3 311.2 %all-gather.13.cloned.1.call-start = ((), (), s32[]{:S(2)}) async-start(), calls=%async_computation.4 | async-start | bytes 2621440 | tf_op jit(solution)/shard_map/all_gather | solution.py:63
  53.1 17.3 %copy-start.34 = (f32[16]{0:T(128)S(1)}, f32[16]{0:T(128)}, u32[]{:S(2)}) copy-start(f32[16]{0:T(128)} %param.24) | copy-start | bytes 196
  53.2 17.4 %copy-start.35 = (u32[128]{0:T(128)S(1)}, u32[128]{0:T(128)}, u32[]{:S(2)}) copy-start(u32[128]{0:T(128)} %constant.147) | copy-start | bytes 1540
  53.2 24.1 %copy-start.30 = (f32[384,2]{0,1:T(2,128)S(1)}, f32[384,2]{0,1:T(2,128)}, u32[]{:S(2)}) copy-start(f32[384,2]{0,1:T(2,128)} %param.25) | copy-start | bytes 9220
  78.6 202.1 %copy-start.13 = (f32[3,2]{1,0:T(4,128)}, f32[3,2]{1,0:T(4,128)S(1)}, u32[]{:S(2)}) copy-start(f32[3,2]{1,0:T(4,128)S(1)} %copy.151) | copy-start | bytes 76
  78.7 202.0 %copy-start.10 = (f32[384,2]{0,1:T(2,128)}, f32[384,2]{0,1:T(2,128)S(1)}, u32[]{:S(2)}) copy-start(f32[384,2]{0,1:T(2,128)S(1)} %copy.178) | copy-start | bytes 9220
  78.9 201.9 %copy-start.12 = (f32[3,2]{1,0:T(4,128)}, f32[3,2]{1,0:T(4,128)S(1)}, u32[]{:S(2)}) copy-start(f32[3,2]{1,0:T(4,128)S(1)} %add_reduce_fusion) | copy-start | bytes 76
  279.4 2.2 collective-permute-start.1
  300.3 0.8 copy-start.1
  301.1 75.2 %all-gather.11.cloned.1.call-start = ((), (), s32[]{:S(2)}) async-start(), calls=%async_computation.3 | async-start | bytes 2621440 | tf_op jit(solution)/shard_map/all_gather | solution.py:63
  302.4 5.0 %copy-start.14 = (f32[2]{0:T(128)S(1)}, f32[2]{0:T(128)}, u32[]{:S(2)}) copy-start(f32[2]{0:T(128)} %get-tuple-element.63) | copy-start | bytes 28
  302.4 33.9 %copy-start.5 = (bf16[2,256,256]{2,1,0:T(8,128)(2,1)S(1)}, bf16[2,256,256]{2,1,0:T(8,128)(2,1)}, u32[]{:S(2)}) copy-start(bf16[2,256,256]{2,1,0:T(8,128)(2,1)} %convert_element_type.135) | copy-start | bytes 786436
  302.5 34.5 %copy-start.20 = (f32[3,2]{1,0:T(4,128)S(1)}, f32[3,2]{1,0:T(4,128)}, u32[]{:S(2)}) copy-start(f32[3,2]{1,0:T(4,128)} %get-tuple-element.65) | copy-start | bytes 76
  302.5 34.5 %copy-start.31 = (f32[3,2]{1,0:T(4,128)S(1)}, f32[3,2]{1,0:T(4,128)}, u32[]{:S(2)}) copy-start(f32[3,2]{1,0:T(4,128)} %get-tuple-element.62) | copy-start | bytes 76
  307.4 33.7 %copy-start.9 = (pred[128,128]{1,0:T(8,128)(4,1)S(1)}, pred[128,128]{1,0:T(8,128)(4,1)}, u32[]{:S(2)}) copy-start(pred[128,128]{1,0:T(8,128)(4,1)} %iota_compare_fusion) | copy-start | bytes 49156
  307.4 33.7 %copy-start.11 = (f32[384,2]{0,1:T(2,128)S(1)}, f32[384,2]{0,1:T(2,128)}, u32[]{:S(2)}) copy-start(f32[384,2]{0,1:T(2,128)} %copy-done.10) | copy-start | bytes 9220
  307.9 35.1 %collective-permute-start = (bf16[16,512]{1,0:T(8,128)(2,1)S(1)}, bf16[16,512]{1,0:T(8,128)(2,1)S(1)}, u32[]{:S(2)}, u32[]{:S(2)}) collective-permute-start(bf16[16,512]{1,0:T(8,128)(2,1)S(1)} %slice.225), channel_id=1, source_target_pairs={{0,8},{8,16},{16,24},{24,32},{32,40},{40,48},{48,56},{56,64},{64,7... | collective-permute-start | bytes 49160 | tf_op jit(solution)/shard_map/ppermute | solution.py:49
  338.3 4.9 %copy-start.21 = (f32[2]{0:T(128)}, f32[2]{0:T(128)S(1)}, u32[]{:S(2)}) copy-start(f32[2]{0:T(128)S(1)} %get-tuple-element.215) | copy-start | bytes 28
  338.3 4.9 %copy-start.23 = (f32[2]{0:T(128)}, f32[2]{0:T(128)S(1)}, u32[]{:S(2)}) copy-start(f32[2]{0:T(128)S(1)} %get-tuple-element.216) | copy-start | bytes 28
  338.3 4.9 %copy-start.24 = (f32[2]{0:T(128)}, f32[2]{0:T(128)S(1)}, u32[]{:S(2)}) copy-start(f32[2]{0:T(128)S(1)} %get-tuple-element.217) | copy-start | bytes 28
  338.3 4.9 %copy-start.25 = (f32[2]{0:T(128)}, f32[2]{0:T(128)S(1)}, u32[]{:S(2)}) copy-start(f32[2]{0:T(128)S(1)} %get-tuple-element.218) | copy-start | bytes 28
  338.3 4.9 %copy-start.26 = (f32[2]{0:T(128)}, f32[2]{0:T(128)S(1)}, u32[]{:S(2)}) copy-start(f32[2]{0:T(128)S(1)} %get-tuple-element.219) | copy-start | bytes 28
  338.3 4.9 %copy-start.27 = (f32[2]{0:T(128)}, f32[2]{0:T(128)S(1)}, u32[]{:S(2)}) copy-start(f32[2]{0:T(128)S(1)} %get-tuple-element.220) | copy-start | bytes 28
  338.3 4.9 %copy-start.28 = (f32[2]{0:T(128)}, f32[2]{0:T(128)S(1)}, u32[]{:S(2)}) copy-start(f32[2]{0:T(128)S(1)} %get-tuple-element.221) | copy-start | bytes 28
  338.3 4.9 %copy-start.29 = (f32[2]{0:T(128)}, f32[2]{0:T(128)S(1)}, u32[]{:S(2)}) copy-start(f32[2]{0:T(128)S(1)} %get-tuple-element.222) | copy-start | bytes 28
  343.5 0.7 copy-start.15
  343.5 0.7 copy-start.16
  343.5 0.7 copy-start.32
  343.5 0.7 copy-start.33
  343.8 1.2 copy-start.18
  345.2 31.1 %copy-start.2 = (f32[8,256,256]{2,1,0:T(8,128)S(1)}, f32[8,256,256]{2,1,0:T(8,128)}, u32[]{:S(2)}) copy-start(f32[8,256,256]{2,1,0:T(8,128)} %all-gather.13.cloned.1.call-done) | copy-start | bytes 6291460
  345.2 31.1 %copy-start.22 = (f32[2]{0:T(128)S(1)}, f32[2]{0:T(128)}, u32[]{:S(2)}) copy-start(f32[2]{0:T(128)} %copy-done.21) | copy-start | bytes 28
  352.1 26.6 %copy-start.6 = (f32[3,128,2,256]{1,3,2,0:T(8,128)S(1)}, f32[3,128,2,256]{1,3,2,0:T(8,128)}, u32[]{:S(2)}) copy-start(f32[3,128,2,256]{1,3,2,0:T(8,128)} %convolution_bitcast_fusion) | copy-start | bytes 2359300
  376.3 2.4 copy-start.3
  381.8 0.8 copy-start.17
Sparse Core Ops, SparseCore 0:
  27.8 30.2 all-gather.8
  301.2 34.6 all-gather.12
  341.2 35.0 all-gather.10
